TPU v7x, 32 devices: a whole 2x2x4 slice. The times are simulated.
32 devices in a mesh: sp: 8 (over z, x), tp: 4 (over y, core).
Axes of the slice: x: 2, y: 2, z: 4, core: 2. Of those that a mesh axis runs over, the one named last changes fastest.
Arguments:
- layer_input: bfloat16 [4, 2048, 2048], P(None, ('sp', 'tp')), as said below
- key_weight: bfloat16 [2048, 384], replicated, may hold values from -0.125 to 0.125
- value_weight: bfloat16 [2048, 384], replicated, may hold values from -0.125 to 0.125
- queries: bfloat16 [24, 5, 64], P('sp'), may hold values from -6 to 6
- head_bias: float32 [6, 5], replicated, as said below
Outputs:
- stored: bfloat16 [24, 8, 256, 128], P('sp', None, 'tp')
- first_read: bfloat16 [24, 320], P('sp')
Inputs may be any that keep to these rules, and one draw needn't show every extreme that they name: `layer_input`: entries lie between -12.5 and 12.5. `head_bias`: entries lie between -1 minus the natural logarithm of 2048 and -3.
All inputs are finite; a program needn't handle non-finite values.
Results may differ from a plain program's by a relative error of at most 0.01.
Values may be sent and summed in bfloat16 or wider, within the bound.
A program may use at most 64 MiB of HBM per device.

v0:
```python
import math
import jax
import jax.numpy as jnp
from jax import lax
from jax.sharding import PartitionSpec as P

HD = 64
KVH = 6
GROUP = 5
EPS_NORM = 0.0001


def head_norm(summed):
    squares = jnp.mean(summed * summed, axis=-1, keepdims=True)
    return summed * lax.rsqrt(squares + EPS_NORM)


def shift_table(pair_ids, head_bias):
    heads_range = jnp.arange(KVH, dtype=jnp.int32)
    picker = (pair_ids[:, None] % KVH == heads_range[None, :]).astype(jnp.float32)
    return jnp.dot(picker, head_bias, precision=lax.Precision.HIGHEST)


def per_device(layer_input, key_weight, value_weight, queries, head_bias):
    seq_count, positions, model_width = layer_input.shape
    tokens_flat = layer_input.reshape(seq_count * positions, model_width)
    key_rows = (
        jnp.dot(tokens_flat, key_weight, preferred_element_type=jnp.float32)
        .astype(jnp.bfloat16)
        .reshape(seq_count, positions, KVH, HD)
    )
    value_rows = (
        jnp.dot(tokens_flat, value_weight, preferred_element_type=jnp.float32)
        .astype(jnp.bfloat16)
        .reshape(seq_count, positions, KVH, HD)
    )
    kv_rows = (
        jnp.concatenate([key_rows, value_rows], axis=-1)
        .transpose(0, 2, 1, 3)
        .reshape(seq_count * KVH, 1, positions, 2 * HD)
    )
    stored = lax.all_to_all(kv_rows, "sp", split_axis=0, concat_axis=1, tiled=True)
    score_scale = 1.0 / math.sqrt(HD)
    local_pairs = queries.shape[0]
    pair_ids = lax.axis_index("sp") * local_pairs + jnp.arange(local_pairs, dtype=jnp.int32)
    head_shift = shift_table(pair_ids, head_bias)
    scores = (
        jnp.einsum("pgc,pbtc->pgbt", queries, stored[..., :HD], preferred_element_type=jnp.float32)
        * score_scale
        + head_shift[:, :, None, None]
    )
    keep_log = jax.nn.log_sigmoid(-scores)
    totals = jnp.sum(keep_log, axis=3)
    gathered = lax.all_gather(totals[None], "tp", axis=0, tiled=True)
    later_mask = (jnp.arange(gathered.shape[0], dtype=jnp.int32) > lax.axis_index("tp")).astype(
        jnp.float32
    )
    later_inside = jnp.sum(gathered * later_mask[:, None, None, None], axis=0)
    block_sums = jnp.sum(gathered, axis=0)
    later_blocks = lax.cumsum(block_sums, axis=2, reverse=True) - block_sums
    suffix_log = (
        lax.cumsum(keep_log, axis=3, reverse=True)
        - keep_log
        + (later_inside + later_blocks)[..., None]
    )
    weights = jnp.exp(jax.nn.log_sigmoid(scores) + suffix_log).astype(jnp.bfloat16)
    partial_value = jnp.einsum(
        "pgbt,pbtc->pgc", weights, stored[..., HD:], preferred_element_type=jnp.float32
    )
    summed = lax.psum(partial_value, "tp")
    first_read = head_norm(summed).reshape(local_pairs, GROUP * HD).astype(jnp.bfloat16)
    return (stored, first_read)


def solution(mesh):
    in_specs = (P(None, ("sp", "tp"), None), P(), P(), P("sp", None, None), P())
    out_specs = (P("sp", None, "tp", None), P("sp", None))
    return jax.shard_map(
        per_device, mesh=mesh, in_specs=in_specs, out_specs=out_specs, check_vma=False
    )
```

profile of v0, /device:TPU:0, one launch (start us, length us, event | category | flops | bytes accessed | tf_op | source)
XLA Modules:
  0.0 53.3 jit_solution(13283465844717739790)
XLA Ops:
  0.6 0.0 copy-start
  0.6 1.4 %copy-done = bf16[2048,384]{1,0:T(8,128)(2,1)S(1)} copy-done((bf16[2048,384]{1,0:T(8,128)(2,1)S(1)}, bf16[2048,384]{1,0:T(8,128)(2,1)}, u32[]{:S(2)}) %copy-start) | copy-done | bytes 1572888
  2.0 0.0 copy-start.2
  2.0 2.0 %convolution_convert_fusion.1 = bf16[256,384]{1,0:T(8,128)(2,1)S(1)} fusion(bf16[256,2048]{1,0:T(8,128)(2,1)} %bitcast.33, bf16[2048,384]{1,0:T(8,128)(2,1)S(1)} %copy-done), kind=kOutput, calls=%fused_computation.1 | convolution fusion | flops 402751488 | bytes 2818048 | tf_op jit(solution)/shard_map/dot_general | solution.py:28
  4.1 0.1 copy.26
  4.2 0.2 reshape.69
  4.4 0.0 copy-done.2
  4.4 2.1 %convolution_convert_fusion = bf16[256,384]{1,0:T(8,128)(2,1)S(1)} fusion(bf16[256,2048]{1,0:T(8,128)(2,1)S(1)} %bitcast.34, bf16[2048,384]{1,0:T(8,128)(2,1)} %param.7), kind=kOutput, calls=%fused_computation | convolution fusion | flops 402751488 | bytes 2818048 | tf_op jit(solution)/shard_map/dot_general | solution.py:33
  6.6 0.1 copy.27
  6.7 0.2 reshape.70
  6.9 0.0 copy-start.4
  6.9 0.6 %maximum_bitcast_fusion = bf16[4,6,64,128]{2,0,3,1:T(4,128)(2,1)S(1)} fusion(bf16[4,64,6,64]{1,0,3,2:T(4,128)(2,1)S(1)} %reshape.70, bf16[4,64,6,64]{1,0,3,2:T(4,128)(2,1)S(1)} %reshape.69), kind=kLoop, calls=%fused_computation.6 | loop fusion | flops 196608 | bytes 786432 | tf_op jit(solution)/shard_map/transpose | solution.py:39
  7.6 0.0 copy-start.3
  7.6 1.2 %copy.28 = bf16[4,6,64,128]{3,2,1,0:T(8,128)(2,1)} copy(bf16[4,6,64,128]{2,0,3,1:T(4,128)(2,1)S(1)} %maximum_bitcast_fusion) | data formatting | bytes 786432 | tf_op jit(solution)/shard_map/transpose | solution.py:39
  8.7 7.3 %all-to-all-start = ((bf16[24,1,64,128]{3,2,1,0:T(8,128)(2,1)}), bf16[24,1,64,128]{3,2,1,0:T(8,128)(2,1)S(1)}, u32[]{:S(2)}, u32[]{:S(2)}) async-start(bf16[24,1,64,128]{3,2,1,0:T(8,128)(2,1)} %bitcast.3), calls=%async_computation | async-start | bytes 786432 | tf_op jit(solution)/shard_map/all_to_all | solution.py:42
  16.0 0.0 copy-done.4
  16.1 0.2 fusion.15
  16.2 11.5 %all-to-all-done = bf16[24,1,64,128]{3,2,1,0:T(8,128)(2,1)S(1)} async-done(((bf16[24,1,64,128]{3,2,1,0:T(8,128)(2,1)}), bf16[24,1,64,128]{3,2,1,0:T(8,128)(2,1)S(1)}, u32[]{:S(2)}, u32[]{:S(2)}) %all-to-all-start) | async-done | bytes 393248 | tf_op jit(solution)/shard_map/all_to_all | solution.py:42
  27.7 0.0 copy-start.1
  27.7 0.0 copy-done.3
  27.8 0.5 fusion.9
  28.3 0.1 copy.34
  28.4 5.2 %all-gather = f32[12,5,8]{2,1,0:T(8,128)S(1)} all-gather(f32[3,5,8]{2,1,0:T(8,128)S(1)} %copy.34), channel_id=2, replica_groups=mesh['sp'=8,'tp'=4] {'tp'}, dimensions={0}, use_global_device_ids=true | all-gather | bytes 2400 | tf_op jit(solution)/shard_map/all_gather | solution.py:54
  33.6 0.1 fusion.19
  33.7 0.5 reduce_window_sum.21
  34.2 0.1 copy.35
  34.3 6.4 %reduce_window_sum.20 = f32[3,5,8,64]{3,2,1,0:T(8,128)S(1)} reduce-window(f32[3,5,8,64]{3,2,1,0:T(8,128)S(1)} %copy.32, f32[]{:T(128)} %constant.36.clone.1), window={size=1x1x1x64 pad=0_0x0_0x0_0x0_63}, to_apply=%region_0.1 | reduce-window | flops 483840 | bytes 61444 | tf_op jit(solution)/shard_map/per_device/reduce_window_sum | solution.py:62
  40.7 0.4 convolution_bitcast_fusion
  41.1 11.4 %psum.7 = f32[3,5,64]{2,1,0:T(8,128)S(1)} all-reduce(f32[3,5,64]{2,1,0:T(8,128)S(1)} %convolution_bitcast_fusion), channel_id=1, replica_groups=mesh['sp'=8,'tp'=4] {'tp'}, use_global_device_ids=true, to_apply=%region_5.6 | all-reduce | flops 960 | bytes 7680 | tf_op jit(solution)/shard_map/psum | solution.py:70
  52.5 0.1 multiply_reduce_fusion.1
  52.6 0.1 multiply_convert_fusion
  52.7 0.7 %convert_element_type.28 = bf16[3,320]{1,0:T(4,128)(2,1)} reshape(bf16[3,5,64]{2,1,0:T(8,128)(2,1)S(1)} %multiply_convert_fusion) | data formatting | bytes 3840 | tf_op jit(solution)/shard_map/convert_element_type | solution.py:71
  53.3 0.0 copy-done.1
  (7 shorter events, 0.1 us)
Async XLA Ops:
  0.6 1.4 %copy-start = (bf16[2048,384]{1,0:T(8,128)(2,1)S(1)}, bf16[2048,384]{1,0:T(8,128)(2,1)}, u32[]{:S(2)}) copy-start(bf16[2048,384]{1,0:T(8,128)(2,1)} %param.6) | copy-start | bytes 4718596
  2.0 2.4 %copy-start.2 = (bf16[4,64,2048]{2,1,0:T(8,128)(2,1)S(1)}, bf16[4,64,2048]{2,1,0:T(8,128)(2,1)}, u32[]{:S(2)}) copy-start(bf16[4,64,2048]{2,1,0:T(8,128)(2,1)} %param.5) | copy-start | bytes 3145732
  6.9 9.1 %copy-start.4 = (f32[6,5]{1,0:T(8,128)S(1)}, f32[6,5]{1,0:T(8,128)}, u32[]{:S(2)}) copy-start(f32[6,5]{1,0:T(8,128)} %param.9) | copy-start | bytes 364
  7.6 20.2 %copy-start.3 = (bf16[3,5,64]{2,0,1:T(4,128)(2,1)S(1)}, bf16[3,5,64]{2,0,1:T(4,128)(2,1)}, u32[]{:S(2)}) copy-start(bf16[3,5,64]{2,0,1:T(4,128)(2,1)} %param.8) | copy-start | bytes 5764
  8.7 19.0 %all-to-all-start = ((bf16[24,1,64,128]{3,2,1,0:T(8,128)(2,1)}), bf16[24,1,64,128]{3,2,1,0:T(8,128)(2,1)S(1)}, u32[]{:S(2)}, u32[]{:S(2)}) async-start(bf16[24,1,64,128]{3,2,1,0:T(8,128)(2,1)} %bitcast.3), calls=%async_computation | async-start | bytes 786432 | tf_op jit(solution)/shard_map/all_to_all | solution.py:42
  27.7 25.6 %copy-start.1 = (bf16[8,3,1,64,128]{4,3,0,1,2:T(8,128)(2,1)}, bf16[8,3,1,64,128]{4,3,0,1,2:T(8,128)(2,1)S(1)}, u32[]{:S(2)}) copy-start(bf16[8,3,1,64,128]{4,3,0,1,2:T(8,128)(2,1)S(1)} %copy.51) | copy-start | bytes 1179652
where the time goes:
time: 53.7 us; the launch traced here: 53.3 us
  blocking collectives  16.6 us (31%)
  waiting for transfers between devices  11.5 us (21%)
  other arithmetic  7.8 us (15%)
  starting transfers between devices  7.28 us (14%)
  matrix products  5.23 us (10%)
  local copies, waits for them, and re-layouts  4.2 us (8%)
  between operations  0.75 us (1%)
    all_to_all x1, waiting for transfers between devices, per_device(): lax.all_to_all(kv_rows, 'sp', split_axis=0, concat_axis=1, tiled=True)  11.5 us
    psum x1, blocking collectives, per_device(): summed = lax.psum(partial_value, 'tp')  11.4 us
    all_to_all x1, starting transfers between devices, per_device(): lax.all_to_all(kv_rows, 'sp', split_axis=0, concat_axis=1, tiled=True)  7.28 us
    another operation x1, other arithmetic, per_device(): lax.cumsum(keep_log, axis=3, reverse=True) - keep_log  6.41 us
    all_gather x1, blocking collectives, per_device(): gathered = lax.all_gather(totals[None], 'tp', axis=0, tiled=True)  5.21 us
    dot_general x1, matrix products, per_device(): jnp.dot(tokens_flat, value_weight, preferred_element_type=jnp.float32)  2.12 us
    dot_general x1, matrix products, per_device(): jnp.dot(tokens_flat, key_weight, preferred_element_type=jnp.float32)  2.02 us
    unnamed x10, local copies, waits for them, and re-layouts  1.43 us
  transfers between devices with their start and end apart: 1, of which 1 were waited for; matrix products, arithmetic and copies ran while one was open for 0% of the time, Pallas kernels for 0%

commit v1 on v0

--- a/solution.py
+++ b/solution.py
@@ -1,3 +1,4 @@
+import functools
 import math
 import jax
 import jax.numpy as jnp
@@ -8,6 +9,18 @@
 KVH = 6
 GROUP = 5
 EPS_NORM = 0.0001
+
+
+def routes_all_apply(here_x, group_axis):
+    extent = lax.axis_size(group_axis)
+    arr_out = lambda y2: [(dev, dev ^ y2) for dev in range(extent)]
+    next_value = here_x
+    for idx in range(extent.bit_length() - 1):
+        next_value = next_value + lax.ppermute(next_value, group_axis, arr_out(1 << idx))
+    return next_value
+
+
+levels_all_switch = functools.partial(routes_all_apply, group_axis="tp")
 
 
 def head_norm(summed):
@@ -67,7 +80,7 @@
     partial_value = jnp.einsum(
         "pgbt,pbtc->pgc", weights, stored[..., HD:], preferred_element_type=jnp.float32
     )
-    summed = lax.psum(partial_value, "tp")
+    summed = levels_all_switch(partial_value)
     first_read = head_norm(summed).reshape(local_pairs, GROUP * HD).astype(jnp.bfloat16)
     return (stored, first_read)
 

time: 53.7 us -> 47.1 us (0.88)
  blocking collectives: 16.6 us -> 5.21 us
  waiting for transfers between devices: 11.5 us -> 14.5 us
  starting transfers between devices: 7.28 us -> 9.18 us
    psum x1 -> x0, blocking collectives: 11.4 us -> none  [per_device(): summed = lax.psum(partial_value, 'tp')]
    ppermute x0 -> x2, waiting for transfers between devices: none -> 3.01 us  [routes_all_apply(): lax.ppermute(next_value, group_axis, arr_out(1 << idx))]
    ppermute x0 -> x2, starting transfers between devices: none -> 1.89 us  [routes_all_apply(): lax.ppermute(next_value, group_axis, arr_out(1 << idx))]
  transfers between devices with their start and end apart: 1 -> 3, of which waited for: 1 -> 3; matrix products, arithmetic and copies ran while one was open for 0% -> 0% of each run, Pallas kernels for 0% -> 0%
where the time goes in v1:
time: 47.1 us; the launch traced here: 46.8 us
  waiting for transfers between devices  14.5 us (31%)
  starting transfers between devices  9.18 us (19%)
  other arithmetic  7.8 us (17%)
  matrix products  5.23 us (11%)
  blocking collectives  5.21 us (11%)
  local copies, waits for them, and re-layouts  4.2 us (9%)
  between operations  0.76 us (2%)
    all_to_all x1, waiting for transfers between devices, per_device(): lax.all_to_all(kv_rows, 'sp', split_axis=0, concat_axis=1, tiled=True)  11.5 us
    all_to_all x1, starting transfers between devices, per_device(): lax.all_to_all(kv_rows, 'sp', split_axis=0, concat_axis=1, tiled=True)  7.28 us
    another operation x1, other arithmetic, per_device(): lax.cumsum(keep_log, axis=3, reverse=True) - keep_log  6.41 us
    all_gather x1, blocking collectives, per_device(): gathered = lax.all_gather(totals[None], 'tp', axis=0, tiled=True)  5.21 us
    ppermute x2, waiting for transfers between devices, routes_all_apply(): lax.ppermute(next_value, group_axis, arr_out(1 << idx))  3.01 us
    dot_general x1, matrix products, per_device(): jnp.dot(tokens_flat, value_weight, preferred_element_type=jnp.float32)  2.12 us
    dot_general x1, matrix products, per_device(): jnp.dot(tokens_flat, key_weight, preferred_element_type=jnp.float32)  2.02 us
    ppermute x2, starting transfers between devices, routes_all_apply(): lax.ppermute(next_value, group_axis, arr_out(1 << idx))  1.89 us
  transfers between devices with their start and end apart: 3, of which 3 were waited for; matrix products, arithmetic and copies ran while one was open for 0% of the time, Pallas kernels for 0%

profile of v1, /device:TPU:0, one launch (start us, length us, event | category | flops | bytes accessed | tf_op | source)
XLA Modules:
  0.0 46.8 jit_solution(7169330504147404881)
XLA Ops:
  0.6 0.0 copy-start
  0.6 1.4 %copy-done = bf16[2048,384]{1,0:T(8,128)(2,1)S(1)} copy-done((bf16[2048,384]{1,0:T(8,128)(2,1)S(1)}, bf16[2048,384]{1,0:T(8,128)(2,1)}, u32[]{:S(2)}) %copy-start) | copy-done | bytes 1572888
  2.0 0.0 copy-start.2
  2.0 2.0 %convolution_convert_fusion.1 = bf16[256,384]{1,0:T(8,128)(2,1)S(1)} fusion(bf16[256,2048]{1,0:T(8,128)(2,1)} %bitcast.33, bf16[2048,384]{1,0:T(8,128)(2,1)S(1)} %copy-done), kind=kOutput, calls=%fused_computation.1 | convolution fusion | flops 402751488 | bytes 2818048 | tf_op jit(solution)/shard_map/dot_general | solution.py:41
  4.1 0.1 copy.26
  4.2 0.2 reshape.69
  4.4 0.0 copy-done.2
  4.4 2.1 %convolution_convert_fusion = bf16[256,384]{1,0:T(8,128)(2,1)S(1)} fusion(bf16[256,2048]{1,0:T(8,128)(2,1)S(1)} %bitcast.34, bf16[2048,384]{1,0:T(8,128)(2,1)} %param.7), kind=kOutput, calls=%fused_computation | convolution fusion | flops 402751488 | bytes 2818048 | tf_op jit(solution)/shard_map/dot_general | solution.py:46
  6.6 0.1 copy.27
  6.7 0.2 reshape.70
  6.9 0.0 copy-start.4
  6.9 0.6 %maximum_bitcast_fusion = bf16[4,6,64,128]{2,0,3,1:T(4,128)(2,1)S(1)} fusion(bf16[4,64,6,64]{1,0,3,2:T(4,128)(2,1)S(1)} %reshape.70, bf16[4,64,6,64]{1,0,3,2:T(4,128)(2,1)S(1)} %reshape.69), kind=kLoop, calls=%fused_computation.6 | loop fusion | flops 196608 | bytes 786432 | tf_op jit(solution)/shard_map/transpose | solution.py:52
  7.6 0.0 copy-start.3
  7.6 1.2 %copy.28 = bf16[4,6,64,128]{3,2,1,0:T(8,128)(2,1)} copy(bf16[4,6,64,128]{2,0,3,1:T(4,128)(2,1)S(1)} %maximum_bitcast_fusion) | data formatting | bytes 786432 | tf_op jit(solution)/shard_map/transpose | solution.py:52
  8.7 7.3 %all-to-all-start = ((bf16[24,1,64,128]{3,2,1,0:T(8,128)(2,1)}), bf16[24,1,64,128]{3,2,1,0:T(8,128)(2,1)S(1)}, u32[]{:S(2)}, u32[]{:S(2)}) async-start(bf16[24,1,64,128]{3,2,1,0:T(8,128)(2,1)} %bitcast.3), calls=%async_computation | async-start | bytes 786432 | tf_op jit(solution)/shard_map/all_to_all | solution.py:55
  16.0 0.0 copy-done.4
  16.1 0.2 fusion.15
  16.2 11.5 %all-to-all-done = bf16[24,1,64,128]{3,2,1,0:T(8,128)(2,1)S(1)} async-done(((bf16[24,1,64,128]{3,2,1,0:T(8,128)(2,1)}), bf16[24,1,64,128]{3,2,1,0:T(8,128)(2,1)S(1)}, u32[]{:S(2)}, u32[]{:S(2)}) %all-to-all-start) | async-done | bytes 393248 | tf_op jit(solution)/shard_map/all_to_all | solution.py:55
  27.7 0.0 copy-start.1
  27.7 0.0 copy-done.3
  27.8 0.5 %fusion.9 = (f32[3,5,8]{1,2,0:T(8,128)S(1)}, f32[3,5,8,64]{3,1,2,0:T(8,128)S(1)}, f32[3,5,8,64]{3,1,2,0:T(8,128)S(1)}) fusion(f32[3,5]{1,0:T(4,128)S(1)} %fusion.15, bf16[3,5,64,1]{2,0,1,3:T(4,128)(2,1)S(1)} %bitcast.35, bf16[3,8,64,128]{3,2,1,0:T(8,128)(2,1)S(1)} %bitcast.29), kind=kOutput, calls=%fused_computation.18 | convolution fusion | flops 1059720 | bytes 457116 | tf_op jit(solution)/shard_map/pgc,pbtc->pgbt/dot_general | solution.py:61
  28.3 0.1 copy.34
  28.4 5.2 %all-gather = f32[12,5,8]{2,1,0:T(8,128)S(1)} all-gather(f32[3,5,8]{2,1,0:T(8,128)S(1)} %copy.34), channel_id=2, replica_groups=mesh['sp'=8,'tp'=4] {'tp'}, dimensions={0}, use_global_device_ids=true | all-gather | bytes 2400 | tf_op jit(solution)/shard_map/all_gather | solution.py:67
  33.6 0.1 fusion.19
  33.7 0.5 %reduce_window_sum.21 = f32[3,5,8]{2,1,0:T(8,128)S(1)} reduce-window(f32[3,5,8]{2,1,0:T(8,128)S(1)} %get-tuple-element.2, f32[]{:T(128)} %constant.36.clone.1), window={size=1x1x8 pad=0_0x0_0x0_7}, to_apply=%region_4.5 | reduce-window | flops 840 | bytes 964 | tf_op jit(solution)/shard_map/per_device/reduce_window_sum | solution.py:73
  34.2 0.1 copy.35
  34.3 6.4 %reduce_window_sum.20 = f32[3,5,8,64]{3,2,1,0:T(8,128)S(1)} reduce-window(f32[3,5,8,64]{3,2,1,0:T(8,128)S(1)} %copy.32, f32[]{:T(128)} %constant.36.clone.1), window={size=1x1x1x64 pad=0_0x0_0x0_0x0_63}, to_apply=%region_0.1 | reduce-window | flops 483840 | bytes 61444 | tf_op jit(solution)/shard_map/per_device/reduce_window_sum | solution.py:75
  40.7 0.4 convolution_bitcast_fusion
  41.1 0.4 collective-permute-start
  41.5 0.8 %collective-permute-done = f32[3,5,64]{2,1,0:T(8,128)S(1)} collective-permute-done((f32[3,5,64]{2,1,0:T(8,128)S(1)}, f32[3,5,64]{2,1,0:T(8,128)S(1)}, u32[]{:S(2)}, u32[]{:S(2)}) %collective-permute-start) | collective-permute-done | bytes 3872 | tf_op jit(solution)/shard_map/ppermute | solution.py:19
  42.3 1.5 %collective-permute-start.1 = (f32[3,5,64]{2,1,0:T(8,128)S(1)}, f32[3,5,64]{2,1,0:T(8,128)S(1)}, u32[]{:S(2)}, u32[]{:S(2)}) collective-permute-start(f32[3,5,64]{2,1,0:T(8,128)S(1)} %add.84), channel_id=1, source_target_pairs={{0,2},{1,3},{2,0},{3,1},{4,6},{5,7},{6,4},{7,5},{8,10},{9,11},{10,... | collective-permute-start | bytes 11528 | tf_op jit(solution)/shard_map/ppermute | solution.py:19
  43.8 2.2 %collective-permute-done.1 = f32[3,5,64]{2,1,0:T(8,128)S(1)} collective-permute-done((f32[3,5,64]{2,1,0:T(8,128)S(1)}, f32[3,5,64]{2,1,0:T(8,128)S(1)}, u32[]{:S(2)}, u32[]{:S(2)}) %collective-permute-start.1) | collective-permute-done | bytes 3872 | tf_op jit(solution)/shard_map/ppermute | solution.py:19
  46.0 0.1 multiply_reduce_fusion.1
  46.1 0.1 multiply_convert_fusion
  46.2 0.7 %convert_element_type.28 = bf16[3,320]{1,0:T(4,128)(2,1)} reshape(bf16[3,5,64]{2,1,0:T(8,128)(2,1)S(1)} %multiply_convert_fusion) | data formatting | bytes 3840 | tf_op jit(solution)/shard_map/convert_element_type | solution.py:84
  46.8 0.0 copy-done.1
  (8 shorter events, 0.1 us)
Async XLA Ops:
  0.6 1.4 %copy-start = (bf16[2048,384]{1,0:T(8,128)(2,1)S(1)}, bf16[2048,384]{1,0:T(8,128)(2,1)}, u32[]{:S(2)}) copy-start(bf16[2048,384]{1,0:T(8,128)(2,1)} %param.6) | copy-start | bytes 4718596
  2.0 2.4 %copy-start.2 = (bf16[4,64,2048]{2,1,0:T(8,128)(2,1)S(1)}, bf16[4,64,2048]{2,1,0:T(8,128)(2,1)}, u32[]{:S(2)}) copy-start(bf16[4,64,2048]{2,1,0:T(8,128)(2,1)} %param.5) | copy-start | bytes 3145732
  6.9 9.1 %copy-start.4 = (f32[6,5]{1,0:T(8,128)S(1)}, f32[6,5]{1,0:T(8,128)}, u32[]{:S(2)}) copy-start(f32[6,5]{1,0:T(8,128)} %param.9) | copy-start | bytes 364
  7.6 20.2 %copy-start.3 = (bf16[3,5,64]{2,0,1:T(4,128)(2,1)S(1)}, bf16[3,5,64]{2,0,1:T(4,128)(2,1)}, u32[]{:S(2)}) copy-start(bf16[3,5,64]{2,0,1:T(4,128)(2,1)} %param.8) | copy-start | bytes 5764
  8.7 19.0 %all-to-all-start = ((bf16[24,1,64,128]{3,2,1,0:T(8,128)(2,1)}), bf16[24,1,64,128]{3,2,1,0:T(8,128)(2,1)S(1)}, u32[]{:S(2)}, u32[]{:S(2)}) async-start(bf16[24,1,64,128]{3,2,1,0:T(8,128)(2,1)} %bitcast.3), calls=%async_computation | async-start | bytes 786432 | tf_op jit(solution)/shard_map/all_to_all | solution.py:55
  27.7 19.1 %copy-start.1 = (bf16[8,3,1,64,128]{4,3,0,1,2:T(8,128)(2,1)}, bf16[8,3,1,64,128]{4,3,0,1,2:T(8,128)(2,1)S(1)}, u32[]{:S(2)}) copy-start(bf16[8,3,1,64,128]{4,3,0,1,2:T(8,128)(2,1)S(1)} %copy.51) | copy-start | bytes 1179652
  41.1 1.2 %collective-permute-start = (f32[3,5,64]{2,1,0:T(8,128)S(1)}, f32[3,5,64]{2,1,0:T(8,128)S(1)}, u32[]{:S(2)}, u32[]{:S(2)}) collective-permute-start(f32[3,5,64]{2,1,0:T(8,128)S(1)} %convolution_bitcast_fusion), channel_id=1, source_target_pairs={{0,1},{1,0},{2,3},{3,2},{4,5},{5,4},{6,7},{7,6},{8,9},{9,8},{10,11... | collective-permute-start | bytes 11528 | tf_op jit(solution)/shard_map/ppermute | solution.py:19
  42.3 3.7 %collective-permute-start.1 = (f32[3,5,64]{2,1,0:T(8,128)S(1)}, f32[3,5,64]{2,1,0:T(8,128)S(1)}, u32[]{:S(2)}, u32[]{:S(2)}) collective-permute-start(f32[3,5,64]{2,1,0:T(8,128)S(1)} %add.84), channel_id=1, source_target_pairs={{0,2},{1,3},{2,0},{3,1},{4,6},{5,7},{6,4},{7,5},{8,10},{9,11},{10,... | collective-permute-start | bytes 11528 | tf_op jit(solution)/shard_map/ppermute | solution.py:19
